TPU v7x, 512 devices: a whole 4x8x8 slice. The times are simulated.
512 devices in a mesh: kv: 64 (over z, y), tp: 8 (over x, core).
Axes of the slice: x: 4, y: 8, z: 8, core: 2. Of those that a mesh axis runs over, the one named last changes fastest.
Arguments:
- tokens: bfloat16 [128, 4096], P(None, 'kv'), may hold values from -16 to 16
- mix_gain: bfloat16 [4096], P('kv'), may hold values from 0.099609375 to 1.8984375
- ffn_gain: bfloat16 [4096], P('kv'), may hold values from 0.099609375 to 1.8984375
- w_query: bfloat16 [4096, 2048], P('kv', 'tp'), may hold values from -0.09375 to 0.09375
- w_key: bfloat16 [4096, 2048], P('kv', 'tp'), may hold values from -0.09375 to 0.09375
- w_value: bfloat16 [4096, 4096], P('kv', 'tp'), may hold values from -0.09375 to 0.09375
- w_gate: bfloat16 [4096, 4096], P('kv', 'tp'), may hold values from -0.09375 to 0.09375
- w_decay: bfloat16 [4096, 2048], P('kv', 'tp'), may hold values from -0.375 to 0.375
- decay_bias: float32 [2048], P('tp'), may hold values from -7 to 4
- head_gain: bfloat16 [512], replicated, may hold values from 0.099609375 to 1.8984375
- w_output: bfloat16 [4096, 4096], P('tp', 'kv'), may hold values from -0.09375 to 0.09375
- w_ffgate: bfloat16 [4096, 11008], P('kv', 'tp'), may hold values from -0.09375 to 0.09375
- w_ffup: bfloat16 [4096, 11008], P('kv', 'tp'), may hold values from -0.09375 to 0.09375
- w_down: bfloat16 [11008, 4096], P('tp', 'kv'), may hold values from -0.0546875 to 0.0546875
- state: float32 [128, 8, 256, 512], P('kv', 'tp'), may hold values from -6 to 6
Outputs:
- mixed: bfloat16 [128, 4096], P(None, 'kv')
- new_state: float32 [128, 8, 256, 512], P('kv', 'tp')
All inputs are finite; a program needn't handle non-finite values.
Results may differ from a plain program's by a relative error of at most 0.015.
Values may be sent and summed in bfloat16 or wider, within the bound.
No kernel may reach another device: no remote copies, remote signals or barrier semaphores. Data moves between devices by JAX's collectives and lax.ppermute only.
A program may use at most 64 MiB of HBM per device.

v0:
```python
import functools

import jax
import jax.numpy as jnp
from jax import lax
from jax.experimental import pallas as pl
from jax.experimental.pallas import tpu as pltpu
from jax.sharding import PartitionSpec as P

epsilon = 1e-06


STRIDE = 8


def member(kv):
    place = kv // STRIDE
    return (place ^ (place >> 2)) & 1


def lines(kv):
    return [[i for i in range(kv) if member(i) == m] for m in range(2)]


def group_order(seqs, kv):
    block = STRIDE * seqs // kv
    places = range(kv // STRIDE)
    order = [i for m in range(2) for i in places if member(i * STRIDE) == m]
    at = lax.broadcasted_iota(jnp.int32, (seqs, seqs), 0)
    source = at
    for i, place in enumerate(order):
        inside = jnp.logical_and(at >= i * block, at < (i + 1) * block)
        source = jnp.where(inside, at + (place - i) * block, source)
    return source == lax.broadcasted_iota(jnp.int32, (seqs, seqs), 1)


def pairs(kv, tp):
    return [
        [i * tp + t for i in sorted((j, j ^ STRIDE), key=member) for t in range(tp)]
        for j in range(kv)
        if j < j ^ STRIDE
    ]


def padded(n):
    return -(-n // 128) * 128


def in_vmem(x):
    return pltpu.with_memory_space_constraint(x, pltpu.VMEM)


def whole(count):
    return [pl.BlockSpec(memory_space=pltpu.VMEM)] * count


def widths(units):
    half = units // 2
    return half, padded(2 * half + 1), padded(half)


def fetch(sources, held, sems):
    copies = [pltpu.make_async_copy(a, b, sems.at[i]) for i, (a, b) in enumerate(zip(sources, held))]
    for c in copies:
        c.start()
    return copies


def project_kernel(*refs, count, kept):
    sources, out_ref = (refs[:count], refs[count])
    held = refs[count + 1 + kept : -1] + refs[count + 1 : count + 1 + kept]
    copies = fetch(sources, held, refs[-1])
    for copy in copies:
        copy.wait()
    tok, gain = held[:2]
    x = tok[...].astype(jnp.float32).T
    mix_in = (x * gain[...].astype(jnp.float32)).astype(jnp.bfloat16)
    at = 0
    for w in held[2 : count - kept]:
        n = w.shape[1]
        part = jnp.dot(mix_in, w[...], preferred_element_type=jnp.float32)
        out_ref[:, at : at + n] = part.astype(jnp.bfloat16)
        at += n
    squares = jnp.sum(x * x, axis=1, keepdims=True)
    rest = out_ref.shape[1] - at
    lane = lax.broadcasted_iota(jnp.int32, (x.shape[0], rest), 1)
    out_ref[:, at:] = jnp.where(lane == 0, squares, 0.0).astype(jnp.bfloat16)


def project(tok_t, gain, weights, kept):
    total = sum(w.shape[1] for w in weights)
    arrays = (tok_t, gain, *weights, *kept)
    return pl.pallas_call(
        functools.partial(project_kernel, count=len(arrays), kept=len(kept)),
        out_shape=(
            pltpu.VMEM((tok_t.shape[1], total + 128), jnp.bfloat16),
            *(pltpu.VMEM(a.shape, a.dtype) for a in kept),
        ),
        in_specs=[pl.BlockSpec(memory_space=pl.ANY)] * len(arrays),
        out_specs=whole(1 + len(kept)),
        scratch_shapes=[pltpu.VMEM(a.shape, a.dtype) for a in arrays[: len(arrays) - len(kept)]]
        + [pltpu.SemaphoreType.DMA((len(arrays),))],
        name="project",
    )(*arrays)


def pack_kernel(_, tok, ffn_gain, *refs):
    splits, (mine_ref, sent_ref, order_ref) = (refs[:-3], refs[-3:])
    rows, units = splits[0].shape
    seqs = tok.shape[1]
    half, both, alone = widths(units)
    order = group_order(seqs, lax.axis_size("kv")).astype(jnp.float32).astype(jnp.bfloat16)
    order_ref[...] = order
    ordered = lax.dot_general(
        tok[...], order, (((1,), (1,)), ((), ())), preferred_element_type=jnp.float32
    ).astype(jnp.bfloat16)

    def fill(ref, m, first):
        gate, up, down = (w[:, m * half : (m + 1) * half] for w in splits)
        ref[:, :half] = gate
        ref[:, half : 2 * half] = up
        ref[:, 2 * half : both] = jnp.zeros((rows, both - 2 * half), ref.dtype)
        ref[:, both : both + half] = down
        ref[:, both + half : both + alone] = jnp.zeros((rows, alone - half), ref.dtype)
        end = both + alone
        ref[:, end : end + seqs] = ordered
        ref[:, end + seqs :] = jnp.zeros((rows, 2 * rows), ref.dtype)
        side = 0 if first else rows
        ref[0:1, end + seqs + side : end + seqs + side + rows] = ffn_gain[...]

    for m in range(2):

        @pl.when(member(lax.axis_index("kv")) == m)
        def _():
            fill(mine_ref, m, True)
            fill(sent_ref, 1 - m, False)


def pack(after, tok_t, ffn_gain, splits):
    width, rows = tok_t.shape
    lanes = sum(widths(splits[0].shape[1])[1:]) + rows + 2 * width
    arrays = (after, tok_t, ffn_gain, *splits)
    return pl.pallas_call(
        pack_kernel,
        out_shape=(
            pltpu.VMEM((width, lanes), jnp.bfloat16),
            pltpu.VMEM((width, lanes), jnp.bfloat16),
            pltpu.VMEM((rows, rows), jnp.bfloat16),
        ),
        in_specs=whole(len(arrays)),
        out_specs=whole(3),
        compiler_params=pltpu.CompilerParams(vmem_limit_bytes=8 << 20),
        name="pack",
    )(*(in_vmem(a) for a in arrays))


def attend_kernel(sums, bias, gain, state, key_ref, value_ref, decay_ref, out_ref, *, model_width):
    rows, _, kd, vd = state.shape
    base = sums[...]
    rms = lax.rsqrt(base[:, 3 * kd + 2 * vd : 3 * kd + 2 * vd + 1] / model_width + epsilon)
    q = base[:, :kd] * rms * kd**-0.5
    k = base[:, kd : 2 * kd] * rms
    v = base[:, 2 * kd : 2 * kd + vd] * rms
    g = base[:, 2 * kd + vd : 2 * kd + 2 * vd] * rms
    x = base[:, 2 * kd + 2 * vd : 3 * kd + 2 * vd] * rms + bias[...]
    log_sigmoid = jnp.minimum(x, 0.0) - jnp.log1p(jnp.exp(-jnp.abs(x)))
    decay = jnp.exp(log_sigmoid / 16.0)
    key_ref[...] = k
    value_ref[...] = v
    decay_ref[...] = decay
    fresh = jnp.sum(q * k, axis=1, keepdims=True) * v
    columns = jnp.concatenate([q * decay, jnp.zeros((8 - rows, kd), jnp.float32)], axis=0).T
    step = 32
    found = []
    for s in range(rows):
        total = jnp.zeros((8, vd), jnp.float32)
        for at in range(0, kd, step):
            read = columns[at : at + step, s : s + 1] * state[s, 0, at : at + step]
            total = total + jnp.sum(read.reshape(step // 8, 8, vd), axis=0)
        found.append(jnp.sum(total, axis=0, keepdims=True))
    attended = jnp.concatenate(found, axis=0) + fresh
    scale = lax.rsqrt(jnp.sum(attended * attended, axis=1, keepdims=True) / vd + epsilon)
    gains = jnp.concatenate([gain[i : i + 1] for i in range(gain.shape[0])], axis=1)
    gated = attended * scale * gains.astype(jnp.float32) * (g / (1.0 + jnp.exp(-g)))
    out_ref[...] = jnp.broadcast_to(gated.astype(jnp.bfloat16)[None], out_ref.shape)


def attend(sums, bias, gain, state, model_width, copies):
    rows, _, kd, vd = state.shape
    return pl.pallas_call(
        functools.partial(attend_kernel, model_width=model_width),
        out_shape=(
            pltpu.VMEM((rows, kd), jnp.float32),
            pltpu.VMEM((rows, vd), jnp.float32),
            pltpu.VMEM((rows, kd), jnp.float32),
            jax.ShapeDtypeStruct((copies, rows, vd), jnp.bfloat16),
        ),
        in_specs=whole(4),
        out_specs=whole(4),
        compiler_params=pltpu.CompilerParams(vmem_limit_bytes=8 << 20),
        name="attend",
    )(*(in_vmem(a) for a in (sums, bias, gain, state)))


def join_kernel(heads, own, other, out_ref, both):
    r = member(lax.axis_index("kv"))
    both[r] = own[...]
    both[1 - r] = other[...]
    weights = both[...].reshape(-1, own.shape[1])
    made = lax.dot_general(
        heads[...], weights, (((1,), (1,)), ((), ())), preferred_element_type=jnp.float32
    ).astype(jnp.bfloat16)
    for j in range(out_ref.shape[0]):
        out_ref[j] = made


def join(heads, own, other, copies):
    return pl.pallas_call(
        join_kernel,
        out_shape=pltpu.VMEM((copies, heads.shape[0], 2 * own.shape[0]), jnp.bfloat16),
        in_specs=whole(3),
        out_specs=pl.BlockSpec(memory_space=pltpu.VMEM),
        scratch_shapes=[pltpu.VMEM((2, *own.shape), own.dtype)],
        compiler_params=pltpu.CompilerParams(vmem_limit_bytes=8 << 20),
        name="join",
    )(*(in_vmem(a) for a in (heads, own, other)))


def total_kernel(parts, out_ref):
    out_ref[...] = jnp.sum(parts[...].astype(jnp.float32), axis=1)


def total(parts):
    return pl.pallas_call(
        total_kernel,
        out_shape=pltpu.VMEM((parts.shape[0], *parts.shape[2:]), jnp.float32),
        in_specs=whole(1),
        out_specs=pl.BlockSpec(memory_space=pltpu.VMEM),
        compiler_params=pltpu.CompilerParams(vmem_limit_bytes=8 << 20),
        name="total",
    )(in_vmem(parts))


def widen_kernel(parts, mine, got, order, _, out_ref, mid_ref, *, alone):
    r = member(lax.axis_index("kv"))
    width, seqs = mid_ref.shape
    both = out_ref.shape[-1]
    end = both + alone
    added = pltpu.roll(parts[...].reshape(seqs, 2 * width), r * width, 1)
    tokens = jnp.concatenate([ref[:, end : end + seqs] for ref in (mine, got)], axis=0)
    x = (tokens.astype(jnp.float32).T + added).astype(jnp.bfloat16).astype(jnp.float32)
    own = x.T[:width].astype(jnp.bfloat16)
    mid_ref[...] = jnp.dot(own, order[...], preferred_element_type=jnp.float32).astype(jnp.bfloat16)
    gains = mine[0:1, end + seqs :].astype(jnp.float32) + got[0:1, end + seqs :].astype(jnp.float32)
    ffn_in = (x * gains).astype(jnp.bfloat16)
    squares = jnp.sum(x * x, axis=1, keepdims=True)
    weights = jnp.concatenate([mine[:, :both], got[:, :both]], axis=0)
    made = jnp.dot(ffn_in, weights, preferred_element_type=jnp.float32)
    lane = lax.broadcasted_iota(jnp.int32, (seqs, 128), 1)
    last = jnp.where(lane == 127, squares, made[:, both - 128 :])
    made = jnp.concatenate([made[:, : both - 128], last], axis=1)
    out_ref[...] = made.reshape(out_ref.shape).astype(jnp.bfloat16)


def widen(parts, mine, got, order, new_state, units, count):
    width, seqs = (mine.shape[0], order.shape[0])
    _, both, alone = widths(units)
    return pl.pallas_call(
        functools.partial(widen_kernel, alone=alone),
        out_shape=(
            pltpu.VMEM((count, seqs // count, both), jnp.bfloat16),
            pltpu.VMEM((width, seqs), jnp.bfloat16),
        ),
        in_specs=whole(5),
        out_specs=whole(2),
        compiler_params=pltpu.CompilerParams(vmem_limit_bytes=8 << 20),
        name="widen",
    )(*(in_vmem(a) for a in (parts, mine, got, order, new_state)))


def gate_kernel(sums, out_ref, *, half, model_width):
    rows, both = sums.shape
    alone = out_ref.shape[-1]
    rms = lax.rsqrt(sums[:, both - 1 :] / model_width + epsilon)
    gate = sums[:, :half] * rms
    up = sums[:, half : 2 * half] * rms
    hidden = gate / (1.0 + jnp.exp(-gate)) * up
    filled = jnp.concatenate([hidden, jnp.zeros((rows, alone - half), jnp.float32)], axis=1)
    out_ref[...] = jnp.broadcast_to(filled.astype(jnp.bfloat16)[None], out_ref.shape)


def gate_units(sums, units, model_width, copies):
    half, _, alone = widths(units)
    return pl.pallas_call(
        functools.partial(gate_kernel, half=half, model_width=model_width),
        out_shape=pltpu.VMEM((copies, sums.shape[0], alone), jnp.bfloat16),
        in_specs=whole(1),
        out_specs=pl.BlockSpec(memory_space=pltpu.VMEM),
        compiler_params=pltpu.CompilerParams(vmem_limit_bytes=8 << 20),
        name="gate",
    )(in_vmem(sums))


def narrow_kernel(hidden, mine, got, order, out_ref, *, both):
    r = member(lax.axis_index("kv"))
    alone = hidden.shape[1]
    copies, width = out_ref.shape[1:3]
    weights = jnp.concatenate([ref[:, both : both + alone] for ref in (mine, got)], axis=0)
    made = lax.dot_general(
        weights, hidden[...], (((1,), (1,)), ((), ())), preferred_element_type=jnp.float32
    ).astype(jnp.bfloat16)
    made = jnp.dot(made, order[...], preferred_element_type=jnp.float32).astype(jnp.bfloat16)
    for j in range(copies):
        out_ref[r, j] = made[:width]
        out_ref[1 - r, j] = made[width:]


def narrow(hidden, mine, got, order, units, tp):
    width, seqs = (mine.shape[0], hidden.shape[0])
    return pl.pallas_call(
        functools.partial(narrow_kernel, both=widths(units)[1]),
        out_shape=pltpu.VMEM((2, tp, width, seqs), jnp.bfloat16),
        in_specs=whole(4),
        out_specs=pl.BlockSpec(memory_space=pltpu.VMEM),
        compiler_params=pltpu.CompilerParams(vmem_limit_bytes=8 << 20),
        name="narrow",
    )(*(in_vmem(a) for a in (hidden, mine, got, order)))


def exchanged(blocks, axis, groups=None):
    return lax.all_to_all(blocks, axis, 0, 0, axis_index_groups=groups, tiled=True)


def summed(blocks):
    return jnp.sum(blocks.astype(jnp.float32), axis=0)


def local(
    tokens,
    mix_gain,
    ffn_gain,
    w_query,
    w_key,
    w_value,
    w_gate,
    w_decay,
    decay_bias,
    head_gain,
    w_output,
    w_ffgate,
    w_ffup,
    w_down,
    state,
):
    own_rows, heads, _, _ = state.shape
    kv, tp = (lax.axis_size(a) for a in ("kv", "tp"))
    model_width = tokens.shape[1] * kv
    made, bias, head_scale, ffn_scale = project(
        tokens.T,
        mix_gain[None, :],
        (w_query, w_key, w_value, w_gate, w_decay),
        (decay_bias[None, :], head_gain.reshape(-1, 128), ffn_gain[None, :]),
    )
    arrived = exchanged(made.reshape(kv, own_rows, -1), "kv")
    pair, line, swap = (pairs(kv, tp), lines(kv), [(i, i ^ STRIDE) for i in range(kv)])
    count = len(line[0])
    seqs, width = tokens.shape
    units = w_ffgate.shape[1]
    keys, values, decay, head_out = attend(
        summed(arrived), bias, head_scale, state, model_width, count
    )
    heads = exchanged(head_out, "kv", line)
    other = lax.ppermute(w_output.T, "kv", swap)
    mine, sent, order = pack(keys, tokens.T, ffn_scale, (w_ffgate, w_ffup, w_down.T))
    got = lax.ppermute(sent, "kv", swap)
    new_state = (
        decay[:, None, :, None] * state + keys[:, None, :, None] * values[:, None, None, :]
    )
    attn_copies = join(heads.reshape(-1, heads.shape[2]), w_output.T, other, 2 * tp)
    attn_copies, new_state = lax.optimization_barrier((attn_copies, new_state))
    attn_parts = exchanged(attn_copies, ("kv", "tp"), pair)
    attn_sums = total(attn_parts.reshape(2, tp, *attn_parts.shape[1:]))
    wide, mid_t = widen(attn_sums, mine, got, order, new_state, units, count)
    sums = summed(exchanged(wide, "kv", line))
    hidden = exchanged(gate_units(sums, units, model_width, count), "kv", line)
    down_parts = narrow(hidden.reshape(seqs, -1), mine, got, order, units, tp)
    down_parts = down_parts.reshape(2 * tp, width, seqs)
    mixed = (
        mid_t.astype(jnp.float32) + summed(exchanged(down_parts, ("kv", "tp"), pair))
    ).astype(jnp.bfloat16)
    return (mixed.T, new_state)


def solution(mesh):
    in_specs = (
        P(None, "kv"),
        P("kv"),
        P("kv"),
        P("kv", "tp"),
        P("kv", "tp"),
        P("kv", "tp"),
        P("kv", "tp"),
        P("kv", "tp"),
        P("tp"),
        P(),
        P("tp", "kv"),
        P("kv", "tp"),
        P("kv", "tp"),
        P("tp", "kv"),
        P("kv", "tp", None, None),
    )
    out_specs = (P(None, "kv"), P("kv", "tp", None, None))
    return jax.shard_map(local, mesh=mesh, in_specs=in_specs, out_specs=out_specs, check_vma=False)
```

profile of v0, /device:TPU:1, one launch (start us, length us, event | category | flops | bytes accessed | tf_op | source)
XLA Modules:
  0.0 125.8 jit_solution(8076842177180292597)
XLA Ops:
  0.6 1.4 %project.1 = (bf16[128,1920]{1,0:T(8,128)(2,1)S(1)}, f32[1,256]{1,0:T(1,128)S(1)}, bf16[4,128]{1,0:T(4,128)(2,1)S(1)}, bf16[1,64]{1,0:T(2,128)(2,1)S(1)}) custom-call(bf16[64,128]{1,0:T(8,128)(2,1)} %bitcast.16, bf16[1,64]{1,0:T(2,128)(2,1)} %bitcast.20, bf16[64,256]{1,0:T(8,128)(2,1)} %refs_2_.1, bf16[64,256]{1,0:T(8,128)(2,1)} %refs_3_.1, ...), custom_call_target="tpu_custom_call" | custom-call | tf_op jit(solution)/shard_map/project/pallas_call | solution.py:93
  2.0 0.0 copy-start.1
  2.0 1.0 reshape.36
  3.0 0.0 copy-start.5
  3.0 17.3 %all-to-all-start = ((bf16[64,2,1920]{2,1,0:T(2,128)(2,1)}), bf16[64,2,1920]{2,1,0:T(2,128)(2,1)S(1)}, u32[]{:S(2)}, u32[]{:S(2)}) async-start(bf16[64,2,1920]{2,1,0:T(2,128)(2,1)} %reshape.36), calls=%async_computation | async-start | bytes 983040 | tf_op jit(solution)/shard_map/all_to_all | solution.py:331
  20.3 0.0 copy-done.5
  20.3 2.9 %collective-permute-start = (bf16[64,512]{1,0:T(8,128)(2,1)S(1)}, bf16[64,512]{1,0:T(8,128)(2,1)S(1)}, u32[]{:S(2)}, u32[]{:S(2)}) collective-permute-start(bf16[64,512]{1,0:T(8,128)(2,1)S(1)} %bitcast.14), channel_id=1, source_target_pairs={{0,64},{8,72},{16,80},{24,88},{32,96},{40,104},{48,112},{56,120},{... | collective-permute-start | bytes 196616 | tf_op jit(solution)/shard_map/ppermute | solution.py:373
  23.2 13.8 %all-to-all-done = bf16[64,2,1920]{2,1,0:T(2,128)(2,1)S(1)} async-done(((bf16[64,2,1920]{2,1,0:T(2,128)(2,1)}), bf16[64,2,1920]{2,1,0:T(2,128)(2,1)S(1)}, u32[]{:S(2)}, u32[]{:S(2)}) %all-to-all-start) | async-done | bytes 491552 | tf_op jit(solution)/shard_map/all_to_all | solution.py:331
  37.0 0.4 convert_reduce_fusion.sums
  37.4 0.0 copy-done.1
  37.4 1.1 attend.1
  38.6 5.6 %all-to-all-start.1 = ((bf16[32,2,512]{2,1,0:T(2,128)(2,1)}), bf16[32,2,512]{2,1,0:T(2,128)(2,1)S(1)}, u32[]{:S(2)}, u32[]{:S(2)}) async-start(bf16[32,2,512]{2,1,0:T(2,128)(2,1)} %get-tuple-element.20), calls=%async_computation.1 | async-start | bytes 131072 | tf_op jit(solution)/shard_map/all_to_all | solution.py:331
  44.2 0.2 multiply_add_fusion._
  44.4 0.0 copy-start
  44.4 10.2 %all-to-all-done.1 = bf16[32,2,512]{2,1,0:T(2,128)(2,1)S(1)} async-done(((bf16[32,2,512]{2,1,0:T(2,128)(2,1)}), bf16[32,2,512]{2,1,0:T(2,128)(2,1)S(1)}, u32[]{:S(2)}, u32[]{:S(2)}) %all-to-all-start.1) | async-done | bytes 65568 | tf_op jit(solution)/shard_map/all_to_all | solution.py:331
  54.6 0.0 collective-permute-done.other
  54.6 0.0 copy-start.4
  54.7 0.9 join.1
  55.6 0.0 copy-start.2
  55.6 0.0 copy-start.3
  55.6 0.0 copy-start.6
  55.6 8.3 %all-to-all-start.2 = ((bf16[16,64,128]{2,1,0:T(8,128)(2,1)}), bf16[16,64,128]{2,1,0:T(8,128)(2,1)S(1)}, u32[]{:S(2)}, u32[]{:S(2)}) async-start(bf16[16,64,128]{2,1,0:T(8,128)(2,1)} %join.1), calls=%async_computation.2 | async-start | bytes 524288 | tf_op jit(solution)/shard_map/all_to_all | solution.py:331
  63.8 0.0 copy-done.4
  63.8 0.0 copy-done.2
  63.9 0.0 copy-done.3
  63.9 0.0 copy-done.6
  63.9 0.2 pack.1
  64.1 3.3 %collective-permute-start.1 = (bf16[64,2432]{1,0:T(8,128)(2,1)S(1)}, bf16[64,2432]{1,0:T(8,128)(2,1)S(1)}, u32[]{:S(2)}, u32[]{:S(2)}) collective-permute-start(bf16[64,2432]{1,0:T(8,128)(2,1)S(1)} %get-tuple-element.27), channel_id=1, source_target_pairs={{0,64},{8,72},{16,80},{24,88},{32,96},{40,104},{48,112},{56,120},{... | collective-permute-start | bytes 933896 | tf_op jit(solution)/shard_map/ppermute | solution.py:375
  67.4 3.6 %all-to-all-done.2 = bf16[16,64,128]{2,1,0:T(8,128)(2,1)S(1)} async-done(((bf16[16,64,128]{2,1,0:T(8,128)(2,1)}), bf16[16,64,128]{2,1,0:T(8,128)(2,1)S(1)}, u32[]{:S(2)}, u32[]{:S(2)}) %all-to-all-start.2) | async-done | bytes 262176 | tf_op jit(solution)/shard_map/all_to_all | solution.py:331
  71.1 4.4 %collective-permute-done.1.got = bf16[64,2432]{1,0:T(8,128)(2,1)S(1)} collective-permute-done((bf16[64,2432]{1,0:T(8,128)(2,1)S(1)}, bf16[64,2432]{1,0:T(8,128)(2,1)S(1)}, u32[]{:S(2)}, u32[]{:S(2)}) %collective-permute-start.1) | collective-permute-done | bytes 311328 | tf_op jit(solution)/shard_map/ppermute | solution.py:375
  75.5 0.4 widen.1
  76.0 0.0 copy-done
  76.0 15.4 %all_to_all.30 = bf16[32,4,1408]{2,1,0:T(4,128)(2,1)S(1)} all-to-all(bf16[32,4,1408]{2,1,0:T(4,128)(2,1)S(1)} %get-tuple-element.31), channel_id=1, replica_groups={{0,8,16,24,32,40,48,56,128,136,144,152,160,168,176,184,320,328,336,344,..., dimensions={0} | all-to-all | bytes 720896 | tf_op jit(solution)/shard_map/all_to_all | solution.py:331
  91.4 0.2 convert_reduce_fusion.1.sums
  91.5 0.2 gate.1
  91.7 18.0 %all_to_all.31 = bf16[32,4,768]{2,1,0:T(4,128)(2,1)S(1)} all-to-all(bf16[32,4,768]{2,1,0:T(4,128)(2,1)S(1)} %gate.1), channel_id=1, replica_groups={{0,8,16,24,32,40,48,56,128,136,144,152,160,168,176,184,320,328,336,344,..., dimensions={0} | all-to-all | bytes 393216 | tf_op jit(solution)/shard_map/all_to_all | solution.py:331
  109.7 0.1 reshape.39.hidden
  109.7 0.3 narrow.1
  110.1 15.1 %all_to_all.32 = bf16[16,64,128]{2,1,0:T(8,128)(2,1)S(1)} all-to-all(bf16[16,64,128]{2,1,0:T(8,128)(2,1)S(1)} %bitcast.11), channel_id=1, replica_groups={{0,1,2,3,4,5,6,7,64,65,66,67,68,69,70,71},{8,9,10,11,12,13,14,15,72,73,..., dimensions={0} | all-to-all | bytes 524288 | tf_op jit(solution)/shard_map/all_to_all | solution.py:331
  125.2 0.6 fusion
  (3 shorter events, 0.1 us)
Async XLA Ops:
  2.0 35.4 %copy-start.1 = (f32[2,1,256,512]{3,2,1,0:T(8,128)S(1)}, f32[2,1,256,512]{3,2,1,0:T(8,128)}, u32[]{:S(2)}) copy-start(f32[2,1,256,512]{3,2,1,0:T(8,128)} %state.1) | copy-start | bytes 3145732
  3.0 17.3 %copy-start.5 = (bf16[512,64]{0,1:T(8,128)(2,1)S(1)}, bf16[512,64]{0,1:T(8,128)(2,1)}, u32[]{:S(2)}) copy-start(bf16[512,64]{0,1:T(8,128)(2,1)} %param.25) | copy-start | bytes 196612
  3.0 34.0 %all-to-all-start = ((bf16[64,2,1920]{2,1,0:T(2,128)(2,1)}), bf16[64,2,1920]{2,1,0:T(2,128)(2,1)S(1)}, u32[]{:S(2)}, u32[]{:S(2)}) async-start(bf16[64,2,1920]{2,1,0:T(2,128)(2,1)} %reshape.36), calls=%async_computation | async-start | bytes 983040 | tf_op jit(solution)/shard_map/all_to_all | solution.py:331
  20.3 34.4 %collective-permute-start = (bf16[64,512]{1,0:T(8,128)(2,1)S(1)}, bf16[64,512]{1,0:T(8,128)(2,1)S(1)}, u32[]{:S(2)}, u32[]{:S(2)}) collective-permute-start(bf16[64,512]{1,0:T(8,128)(2,1)S(1)} %bitcast.14), channel_id=1, source_target_pairs={{0,64},{8,72},{16,80},{24,88},{32,96},{40,104},{48,112},{56,120},{... | collective-permute-start | bytes 196616 | tf_op jit(solution)/shard_map/ppermute | solution.py:373
  38.6 16.0 %all-to-all-start.1 = ((bf16[32,2,512]{2,1,0:T(2,128)(2,1)}), bf16[32,2,512]{2,1,0:T(2,128)(2,1)S(1)}, u32[]{:S(2)}, u32[]{:S(2)}) async-start(bf16[32,2,512]{2,1,0:T(2,128)(2,1)} %get-tuple-element.20), calls=%async_computation.1 | async-start | bytes 131072 | tf_op jit(solution)/shard_map/all_to_all | solution.py:331
  44.4 31.5 %copy-start = (f32[2,1,256,512]{3,2,1,0:T(8,128)}, f32[2,1,256,512]{3,2,1,0:T(8,128)S(1)}, u32[]{:S(2)}) copy-start(f32[2,1,256,512]{3,2,1,0:T(8,128)S(1)} %multiply_add_fusion._) | copy-start | bytes 3145732
  54.6 9.2 %copy-start.4 = (bf16[1376,64]{0,1:T(8,128)(2,1)S(1)}, bf16[1376,64]{0,1:T(8,128)(2,1)}, u32[]{:S(2)}) copy-start(bf16[1376,64]{0,1:T(8,128)(2,1)} %param.28) | copy-start | bytes 528388
  55.6 8.3 %copy-start.2 = (bf16[64,1376]{1,0:T(8,128)(2,1)S(1)}, bf16[64,1376]{1,0:T(8,128)(2,1)}, u32[]{:S(2)}) copy-start(bf16[64,1376]{1,0:T(8,128)(2,1)} %refs_0_.1) | copy-start | bytes 528388
  55.6 8.3 %copy-start.3 = (bf16[64,1376]{1,0:T(8,128)(2,1)S(1)}, bf16[64,1376]{1,0:T(8,128)(2,1)}, u32[]{:S(2)}) copy-start(bf16[64,1376]{1,0:T(8,128)(2,1)} %refs_1_.1) | copy-start | bytes 528388
  55.6 8.3 %copy-start.6 = (bf16[128,64]{0,1:T(8,128)(2,1)S(1)}, bf16[128,64]{0,1:T(8,128)(2,1)}, u32[]{:S(2)}) copy-start(bf16[128,64]{0,1:T(8,128)(2,1)} %param.15) | copy-start | bytes 49156
  55.6 15.5 %all-to-all-start.2 = ((bf16[16,64,128]{2,1,0:T(8,128)(2,1)}), bf16[16,64,128]{2,1,0:T(8,128)(2,1)S(1)}, u32[]{:S(2)}, u32[]{:S(2)}) async-start(bf16[16,64,128]{2,1,0:T(8,128)(2,1)} %join.1), calls=%async_computation.2 | async-start | bytes 524288 | tf_op jit(solution)/shard_map/all_to_all | solution.py:331
  64.1 11.4 %collective-permute-start.1 = (bf16[64,2432]{1,0:T(8,128)(2,1)S(1)}, bf16[64,2432]{1,0:T(8,128)(2,1)S(1)}, u32[]{:S(2)}, u32[]{:S(2)}) collective-permute-start(bf16[64,2432]{1,0:T(8,128)(2,1)S(1)} %get-tuple-element.27), channel_id=1, source_target_pairs={{0,64},{8,72},{16,80},{24,88},{32,96},{40,104},{48,112},{56,120},{... | collective-permute-start | bytes 933896 | tf_op jit(solution)/shard_map/ppermute | solution.py:375
where the time goes:
time: 126 us
  blocking collectives  48.4 us (38%)
  starting transfers between devices  37.4 us (30%)
  waiting for transfers between devices  32 us (25%)
  Pallas kernels  4.61 us (4%)
  other arithmetic  1.44 us (1%)
    all_to_all x3, blocking collectives, exchanged(): lax.all_to_all(blocks, axis, 0, 0, axis_index_groups=groups, tiled=True)  48.4 us
    all_to_all x3, starting transfers between devices, exchanged(): lax.all_to_all(blocks, axis, 0, 0, axis_index_groups=groups, tiled=True)  31.1 us
    all_to_all x3, waiting for transfers between devices, exchanged(): lax.all_to_all(blocks, axis, 0, 0, axis_index_groups=groups, tiled=True)  27.6 us
    ppermute x1, waiting for transfers between devices, local(): got = lax.ppermute(sent, 'kv', swap)  4.43 us
    ppermute x1, starting transfers between devices, local(): got = lax.ppermute(sent, 'kv', swap)  3.35 us
    ppermute x1, starting transfers between devices, local(): other = lax.ppermute(w_output.T, 'kv', swap)  2.92 us
  transfers between devices with their start and end apart: 5, of which 4 were waited for; matrix products, arithmetic and copies ran while one was open for 1% of the time, Pallas kernels for 1%

commit v1 on v0

--- a/solution.py
+++ b/solution.py
@@ -105,7 +105,10 @@
 
 
 def pack_kernel(_, tok, ffn_gain, *refs):
-    splits, (mine_ref, sent_ref, order_ref) = (refs[:-3], refs[-3:])
+    splits, (mine_ref, sent_ref, down_ref, order_ref) = (
+        refs[:-4],
+        refs[-4:],
+    )
     rows, units = splits[0].shape
     seqs = tok.shape[1]
     half, both, alone = widths(units)
@@ -120,13 +123,14 @@
         ref[:, :half] = gate
         ref[:, half : 2 * half] = up
         ref[:, 2 * half : both] = jnp.zeros((rows, both - 2 * half), ref.dtype)
-        ref[:, both : both + half] = down
-        ref[:, both + half : both + alone] = jnp.zeros((rows, alone - half), ref.dtype)
-        end = both + alone
-        ref[:, end : end + seqs] = ordered
-        ref[:, end + seqs :] = jnp.zeros((rows, 2 * rows), ref.dtype)
-        side = 0 if first else rows
-        ref[0:1, end + seqs + side : end + seqs + side + rows] = ffn_gain[...]
+        ref[:, both : both + seqs] = ordered
+        end = both + seqs + 2 * rows
+        ref[:, both + seqs : end] = jnp.zeros((rows, 2 * rows), ref.dtype)
+        side = both + seqs + (0 if first else rows)
+        ref[0:1, side : side + rows] = ffn_gain[...]
+        down_to, at = (ref, end) if first else (down_ref, 0)
+        down_to[:, at : at + half] = down
+        down_to[:, at + half : at + alone] = jnp.zeros((rows, alone - half), ref.dtype)
 
     for m in range(2):
 
@@ -138,17 +142,19 @@
 
 def pack(after, tok_t, ffn_gain, splits):
     width, rows = tok_t.shape
-    lanes = sum(widths(splits[0].shape[1])[1:]) + rows + 2 * width
+    _, both, alone = widths(splits[0].shape[1])
+    lanes = both + rows + 2 * width
     arrays = (after, tok_t, ffn_gain, *splits)
     return pl.pallas_call(
         pack_kernel,
         out_shape=(
+            pltpu.VMEM((width, lanes + alone), jnp.bfloat16),
             pltpu.VMEM((width, lanes), jnp.bfloat16),
-            pltpu.VMEM((width, lanes), jnp.bfloat16),
+            pltpu.VMEM((width, alone), jnp.bfloat16),
             pltpu.VMEM((rows, rows), jnp.bfloat16),
         ),
         in_specs=whole(len(arrays)),
-        out_specs=whole(3),
+        out_specs=whole(4),
         compiler_params=pltpu.CompilerParams(vmem_limit_bytes=8 << 20),
         name="pack",
     )(*(in_vmem(a) for a in arrays))
@@ -241,17 +247,18 @@
     )(in_vmem(parts))
 
 
-def widen_kernel(parts, mine, got, order, _, out_ref, mid_ref, *, alone):
+def widen_kernel(parts, mine, got, order, _, out_ref, mid_ref):
     r = member(lax.axis_index("kv"))
     width, seqs = mid_ref.shape
     both = out_ref.shape[-1]
-    end = both + alone
+    end = both
     added = pltpu.roll(parts[...].reshape(seqs, 2 * width), r * width, 1)
     tokens = jnp.concatenate([ref[:, end : end + seqs] for ref in (mine, got)], axis=0)
     x = (tokens.astype(jnp.float32).T + added).astype(jnp.bfloat16).astype(jnp.float32)
     own = x.T[:width].astype(jnp.bfloat16)
     mid_ref[...] = jnp.dot(own, order[...], preferred_element_type=jnp.float32).astype(jnp.bfloat16)
-    gains = mine[0:1, end + seqs :].astype(jnp.float32) + got[0:1, end + seqs :].astype(jnp.float32)
+    row = slice(end + seqs, end + seqs + 2 * width)
+    gains = mine[0:1, row].astype(jnp.float32) + got[0:1, row].astype(jnp.float32)
     ffn_in = (x * gains).astype(jnp.bfloat16)
     squares = jnp.sum(x * x, axis=1, keepdims=True)
     weights = jnp.concatenate([mine[:, :both], got[:, :both]], axis=0)
@@ -264,9 +271,9 @@
 
 def widen(parts, mine, got, order, new_state, units, count):
     width, seqs = (mine.shape[0], order.shape[0])
-    _, both, alone = widths(units)
-    return pl.pallas_call(
-        functools.partial(widen_kernel, alone=alone),
+    both = widths(units)[1]
+    return pl.pallas_call(
+        widen_kernel,
         out_shape=(
             pltpu.VMEM((count, seqs // count, both), jnp.bfloat16),
             pltpu.VMEM((width, seqs), jnp.bfloat16),
@@ -301,11 +308,11 @@
     )(in_vmem(sums))
 
 
-def narrow_kernel(hidden, mine, got, order, out_ref, *, both):
+def narrow_kernel(hidden, mine, got, order, out_ref):
     r = member(lax.axis_index("kv"))
     alone = hidden.shape[1]
     copies, width = out_ref.shape[1:3]
-    weights = jnp.concatenate([ref[:, both : both + alone] for ref in (mine, got)], axis=0)
+    weights = jnp.concatenate([mine[:, mine.shape[1] - alone :], got[...]], axis=0)
     made = lax.dot_general(
         weights, hidden[...], (((1,), (1,)), ((), ())), preferred_element_type=jnp.float32
     ).astype(jnp.bfloat16)
@@ -315,10 +322,10 @@
         out_ref[1 - r, j] = made[width:]
 
 
-def narrow(hidden, mine, got, order, units, tp):
+def narrow(hidden, mine, got, order, tp):
     width, seqs = (mine.shape[0], hidden.shape[0])
     return pl.pallas_call(
-        functools.partial(narrow_kernel, both=widths(units)[1]),
+        narrow_kernel,
         out_shape=pltpu.VMEM((2, tp, width, seqs), jnp.bfloat16),
         in_specs=whole(4),
         out_specs=pl.BlockSpec(memory_space=pltpu.VMEM),
@@ -371,8 +378,9 @@
     )
     heads = exchanged(head_out, "kv", line)
     other = lax.ppermute(w_output.T, "kv", swap)
-    mine, sent, order = pack(keys, tokens.T, ffn_scale, (w_ffgate, w_ffup, w_down.T))
+    mine, sent, sent_down, order = pack(keys, tokens.T, ffn_scale, (w_ffgate, w_ffup, w_down.T))
     got = lax.ppermute(sent, "kv", swap)
+    got_down = lax.ppermute(sent_down, "kv", swap)
     new_state = (
         decay[:, None, :, None] * state + keys[:, None, :, None] * values[:, None, None, :]
     )
@@ -382,8 +390,10 @@
     attn_sums = total(attn_parts.reshape(2, tp, *attn_parts.shape[1:]))
     wide, mid_t = widen(attn_sums, mine, got, order, new_state, units, count)
     sums = summed(exchanged(wide, "kv", line))
-    hidden = exchanged(gate_units(sums, units, model_width, count), "kv", line)
-    down_parts = narrow(hidden.reshape(seqs, -1), mine, got, order, units, tp)
+    hidden = gate_units(sums, units, model_width, count)
+    hidden, got_down = lax.optimization_barrier((hidden, got_down))
+    hidden = exchanged(hidden, "kv", line)
+    down_parts = narrow(hidden.reshape(seqs, -1), mine, got_down, order, tp)
     down_parts = down_parts.reshape(2 * tp, width, seqs)
     mixed = (
         mid_t.astype(jnp.float32) + summed(exchanged(down_parts, ("kv", "tp"), pair))

time: 126 us -> 126 us (level)
  blocking collectives: 48.4 us -> 33.1 us
  waiting for transfers between devices: 32 us -> 40.3 us
  starting transfers between devices: 37.4 us -> 43.6 us
    all_to_all x3 -> x2, blocking collectives: 48.4 us -> 33.1 us  [exchanged(): lax.all_to_all(blocks, axis, 0, 0, axis_index_groups=groups, tiled=True)]
    all_to_all x3 -> x4, waiting for transfers between devices: 27.6 us -> 38 us  [exchanged(): lax.all_to_all(blocks, axis, 0, 0, axis_index_groups=groups, tiled=True)]
    all_to_all x3 -> x4, starting transfers between devices: 31.1 us -> 35 us  [exchanged(): lax.all_to_all(blocks, axis, 0, 0, axis_index_groups=groups, tiled=True)]
    ppermute x0 -> x1, starting transfers between devices: none -> 2.32 us  [local(): got_down = lax.ppermute(sent_down, 'kv', swap)]
    ppermute x1, waiting for transfers between devices: 4.43 us -> 2.32 us  [local(): got = lax.ppermute(sent, 'kv', swap)]
  transfers between devices with their start and end apart: 5 -> 7, of which waited for: 4 -> 5; matrix products, arithmetic and copies ran while one was open for 1% -> 1% of each run, Pallas kernels for 1% -> 1%
where the time goes in v1:
time: 126 us
  starting transfers between devices  43.6 us (35%)
  waiting for transfers between devices  40.3 us (32%)
  blocking collectives  33.1 us (26%)
  Pallas kernels  5.31 us (4%)
  other arithmetic  1.44 us (1%)
    all_to_all x4, waiting for transfers between devices, exchanged(): lax.all_to_all(blocks, axis, 0, 0, axis_index_groups=groups, tiled=True)  38 us
    all_to_all x4, starting transfers between devices, exchanged(): lax.all_to_all(blocks, axis, 0, 0, axis_index_groups=groups, tiled=True)  35 us
    all_to_all x2, blocking collectives, exchanged(): lax.all_to_all(blocks, axis, 0, 0, axis_index_groups=groups, tiled=True)  33.1 us
    ppermute x1, starting transfers between devices, local(): got = lax.ppermute(sent, 'kv', swap)  3.35 us
    ppermute x1, starting transfers between devices, local(): other = lax.ppermute(w_output.T, 'kv', swap)  2.92 us
  transfers between devices with their start and end apart: 7, of which 5 were waited for; matrix products, arithmetic and copies ran while one was open for 1% of the time, Pallas kernels for 1%

profile of v1, /device:TPU:1, one launch (start us, length us, event | category | flops | bytes accessed | tf_op | source)
XLA Modules:
  0.0 125.7 jit_solution(8593701965199569893)
XLA Ops:
  0.6 1.4 %project.1 = (bf16[128,1920]{1,0:T(8,128)(2,1)S(1)}, f32[1,256]{1,0:T(1,128)S(1)}, bf16[4,128]{1,0:T(4,128)(2,1)S(1)}, bf16[1,64]{1,0:T(2,128)(2,1)S(1)}) custom-call(bf16[64,128]{1,0:T(8,128)(2,1)} %bitcast.16, bf16[1,64]{1,0:T(2,128)(2,1)} %bitcast.20, bf16[64,256]{1,0:T(8,128)(2,1)} %refs_2_.1, bf16[64,256]{1,0:T(8,128)(2,1)} %refs_3_.1, ...), custom_call_target="tpu_custom_call" | custom-call | tf_op jit(solution)/shard_map/project/pallas_call | solution.py:93
  2.0 0.0 copy-start
  2.0 1.0 reshape.36
  3.0 0.0 copy-start.5
  3.0 17.3 %all-to-all-start = ((bf16[64,2,1920]{2,1,0:T(2,128)(2,1)}), bf16[64,2,1920]{2,1,0:T(2,128)(2,1)S(1)}, u32[]{:S(2)}, u32[]{:S(2)}) async-start(bf16[64,2,1920]{2,1,0:T(2,128)(2,1)} %reshape.36), calls=%async_computation | async-start | bytes 983040 | tf_op jit(solution)/shard_map/all_to_all | solution.py:338
  20.3 0.0 copy-done.5
  20.3 2.9 %collective-permute-start = (bf16[64,512]{1,0:T(8,128)(2,1)S(1)}, bf16[64,512]{1,0:T(8,128)(2,1)S(1)}, u32[]{:S(2)}, u32[]{:S(2)}) collective-permute-start(bf16[64,512]{1,0:T(8,128)(2,1)S(1)} %bitcast.14), channel_id=1, source_target_pairs={{0,64},{8,72},{16,80},{24,88},{32,96},{40,104},{48,112},{56,120},{... | collective-permute-start | bytes 196616 | tf_op jit(solution)/shard_map/ppermute | solution.py:380
  23.2 13.8 %all-to-all-done = bf16[64,2,1920]{2,1,0:T(2,128)(2,1)S(1)} async-done(((bf16[64,2,1920]{2,1,0:T(2,128)(2,1)}), bf16[64,2,1920]{2,1,0:T(2,128)(2,1)S(1)}, u32[]{:S(2)}, u32[]{:S(2)}) %all-to-all-start) | async-done | bytes 491552 | tf_op jit(solution)/shard_map/all_to_all | solution.py:338
  37.0 0.4 convert_reduce_fusion.sums
  37.4 0.0 copy-done
  37.4 1.1 attend.1
  38.6 5.6 %all-to-all-start.1 = ((bf16[32,2,512]{2,1,0:T(2,128)(2,1)}), bf16[32,2,512]{2,1,0:T(2,128)(2,1)S(1)}, u32[]{:S(2)}, u32[]{:S(2)}) async-start(bf16[32,2,512]{2,1,0:T(2,128)(2,1)} %get-tuple-element.23), calls=%async_computation.1 | async-start | bytes 131072 | tf_op jit(solution)/shard_map/all_to_all | solution.py:338
  44.2 0.2 multiply_add_fusion._
  44.4 0.0 copy-start.1
  44.4 10.2 %all-to-all-done.1 = bf16[32,2,512]{2,1,0:T(2,128)(2,1)S(1)} async-done(((bf16[32,2,512]{2,1,0:T(2,128)(2,1)}), bf16[32,2,512]{2,1,0:T(2,128)(2,1)S(1)}, u32[]{:S(2)}, u32[]{:S(2)}) %all-to-all-start.1) | async-done | bytes 65568 | tf_op jit(solution)/shard_map/all_to_all | solution.py:338
  54.6 0.0 collective-permute-done.other
  54.6 0.0 copy-start.4
  54.7 0.9 join.1
  55.6 0.0 copy-start.2
  55.6 0.0 copy-start.3
  55.6 0.0 copy-start.6
  55.6 8.3 %all-to-all-start.2 = ((bf16[16,64,128]{2,1,0:T(8,128)(2,1)}), bf16[16,64,128]{2,1,0:T(8,128)(2,1)S(1)}, u32[]{:S(2)}, u32[]{:S(2)}) async-start(bf16[16,64,128]{2,1,0:T(8,128)(2,1)} %join.1), calls=%async_computation.2 | async-start | bytes 524288 | tf_op jit(solution)/shard_map/all_to_all | solution.py:338
  63.8 0.0 copy-done.4
  63.8 0.0 copy-done.2
  63.8 0.0 copy-done.3
  63.8 0.0 copy-done.6
  63.9 0.2 pack.1
  64.1 3.3 %collective-permute-start.1 = (bf16[64,1664]{1,0:T(8,128)(2,1)S(1)}, bf16[64,1664]{1,0:T(8,128)(2,1)S(1)}, u32[]{:S(2)}, u32[]{:S(2)}) collective-permute-start(bf16[64,1664]{1,0:T(8,128)(2,1)S(1)} %get-tuple-element.30), channel_id=1, source_target_pairs={{0,64},{8,72},{16,80},{24,88},{32,96},{40,104},{48,112},{56,120},{... | collective-permute-start | bytes 638984 | tf_op jit(solution)/shard_map/ppermute | solution.py:382
  67.4 3.6 %all-to-all-done.2 = bf16[16,64,128]{2,1,0:T(8,128)(2,1)S(1)} async-done(((bf16[16,64,128]{2,1,0:T(8,128)(2,1)}), bf16[16,64,128]{2,1,0:T(8,128)(2,1)S(1)}, u32[]{:S(2)}, u32[]{:S(2)}) %all-to-all-start.2) | async-done | bytes 262176 | tf_op jit(solution)/shard_map/all_to_all | solution.py:338
  71.1 2.3 %collective-permute-done.1.got = bf16[64,1664]{1,0:T(8,128)(2,1)S(1)} collective-permute-done((bf16[64,1664]{1,0:T(8,128)(2,1)S(1)}, bf16[64,1664]{1,0:T(8,128)(2,1)S(1)}, u32[]{:S(2)}, u32[]{:S(2)}) %collective-permute-start.1) | collective-permute-done | bytes 213024 | tf_op jit(solution)/shard_map/ppermute | solution.py:382
  73.4 1.1 widen.1
  74.6 0.0 copy-done.1
  74.6 3.9 %all-to-all-start.3 = ((bf16[32,4,1408]{2,1,0:T(4,128)(2,1)}), bf16[32,4,1408]{2,1,0:T(4,128)(2,1)S(1)}, u32[]{:S(2)}, u32[]{:S(2)}) async-start(bf16[32,4,1408]{2,1,0:T(4,128)(2,1)} %get-tuple-element.34), calls=%async_computation.3 | async-start | bytes 720896 | tf_op jit(solution)/shard_map/all_to_all | solution.py:338
  78.4 2.3 %collective-permute-start.2 = (bf16[64,768]{1,0:T(8,128)(2,1)S(1)}, bf16[64,768]{1,0:T(8,128)(2,1)S(1)}, u32[]{:S(2)}, u32[]{:S(2)}) collective-permute-start(bf16[64,768]{1,0:T(8,128)(2,1)S(1)} %get-tuple-element.35), channel_id=1, source_target_pairs={{0,64},{8,72},{16,80},{24,88},{32,96},{40,104},{48,112},{56,120},{... | collective-permute-start | bytes 294920 | tf_op jit(solution)/shard_map/ppermute | solution.py:383
  80.8 10.4 %all-to-all-done.3 = bf16[32,4,1408]{2,1,0:T(4,128)(2,1)S(1)} async-done(((bf16[32,4,1408]{2,1,0:T(4,128)(2,1)}), bf16[32,4,1408]{2,1,0:T(4,128)(2,1)S(1)}, u32[]{:S(2)}, u32[]{:S(2)}) %all-to-all-start.3) | async-done | bytes 360480 | tf_op jit(solution)/shard_map/all_to_all | solution.py:338
  91.2 0.2 convert_reduce_fusion.1.sums
  91.4 0.2 gate.1
  91.5 0.0 collective-permute-done.2.got
  91.5 18.2 %all_to_all.30 = bf16[32,4,768]{2,1,0:T(4,128)(2,1)S(1)} all-to-all(bf16[32,4,768]{2,1,0:T(4,128)(2,1)S(1)} %gate.1), channel_id=1, replica_groups={{0,8,16,24,32,40,48,56,128,136,144,152,160,168,176,184,320,328,336,344,..., dimensions={0} | all-to-all | bytes 393216 | tf_op jit(solution)/shard_map/all_to_all | solution.py:338
  109.8 0.1 reshape.39.hidden
  109.8 0.3 narrow.1
  110.2 14.8 %all_to_all.31 = bf16[16,64,128]{2,1,0:T(8,128)(2,1)S(1)} all-to-all(bf16[16,64,128]{2,1,0:T(8,128)(2,1)S(1)} %bitcast.11), channel_id=1, replica_groups={{0,1,2,3,4,5,6,7,64,65,66,67,68,69,70,71},{8,9,10,11,12,13,14,15,72,73,..., dimensions={0} | all-to-all | bytes 524288 | tf_op jit(solution)/shard_map/all_to_all | solution.py:338
  125.1 0.6 fusion
  (3 shorter events, 0.1 us)
Async XLA Ops:
  2.0 35.4 %copy-start = (f32[2,1,256,512]{3,2,1,0:T(8,128)S(1)}, f32[2,1,256,512]{3,2,1,0:T(8,128)}, u32[]{:S(2)}) copy-start(f32[2,1,256,512]{3,2,1,0:T(8,128)} %state.1) | copy-start | bytes 3145732
  3.0 17.3 %copy-start.5 = (bf16[512,64]{0,1:T(8,128)(2,1)S(1)}, bf16[512,64]{0,1:T(8,128)(2,1)}, u32[]{:S(2)}) copy-start(bf16[512,64]{0,1:T(8,128)(2,1)} %param.25) | copy-start | bytes 196612
  3.0 34.0 %all-to-all-start = ((bf16[64,2,1920]{2,1,0:T(2,128)(2,1)}), bf16[64,2,1920]{2,1,0:T(2,128)(2,1)S(1)}, u32[]{:S(2)}, u32[]{:S(2)}) async-start(bf16[64,2,1920]{2,1,0:T(2,128)(2,1)} %reshape.36), calls=%async_computation | async-start | bytes 983040 | tf_op jit(solution)/shard_map/all_to_all | solution.py:338
  20.3 34.4 %collective-permute-start = (bf16[64,512]{1,0:T(8,128)(2,1)S(1)}, bf16[64,512]{1,0:T(8,128)(2,1)S(1)}, u32[]{:S(2)}, u32[]{:S(2)}) collective-permute-start(bf16[64,512]{1,0:T(8,128)(2,1)S(1)} %bitcast.14), channel_id=1, source_target_pairs={{0,64},{8,72},{16,80},{24,88},{32,96},{40,104},{48,112},{56,120},{... | collective-permute-start | bytes 196616 | tf_op jit(solution)/shard_map/ppermute | solution.py:380
  38.6 16.0 %all-to-all-start.1 = ((bf16[32,2,512]{2,1,0:T(2,128)(2,1)}), bf16[32,2,512]{2,1,0:T(2,128)(2,1)S(1)}, u32[]{:S(2)}, u32[]{:S(2)}) async-start(bf16[32,2,512]{2,1,0:T(2,128)(2,1)} %get-tuple-element.23), calls=%async_computation.1 | async-start | bytes 131072 | tf_op jit(solution)/shard_map/all_to_all | solution.py:338
  44.4 30.1 %copy-start.1 = (f32[2,1,256,512]{3,2,1,0:T(8,128)}, f32[2,1,256,512]{3,2,1,0:T(8,128)S(1)}, u32[]{:S(2)}) copy-start(f32[2,1,256,512]{3,2,1,0:T(8,128)S(1)} %multiply_add_fusion._) | copy-start | bytes 3145732
  54.6 9.2 %copy-start.4 = (bf16[1376,64]{0,1:T(8,128)(2,1)S(1)}, bf16[1376,64]{0,1:T(8,128)(2,1)}, u32[]{:S(2)}) copy-start(bf16[1376,64]{0,1:T(8,128)(2,1)} %param.28) | copy-start | bytes 528388
  55.6 8.3 %copy-start.2 = (bf16[64,1376]{1,0:T(8,128)(2,1)S(1)}, bf16[64,1376]{1,0:T(8,128)(2,1)}, u32[]{:S(2)}) copy-start(bf16[64,1376]{1,0:T(8,128)(2,1)} %refs_0_.1) | copy-start | bytes 528388
  55.6 8.3 %copy-start.3 = (bf16[64,1376]{1,0:T(8,128)(2,1)S(1)}, bf16[64,1376]{1,0:T(8,128)(2,1)}, u32[]{:S(2)}) copy-start(bf16[64,1376]{1,0:T(8,128)(2,1)} %refs_1_.1) | copy-start | bytes 528388
  55.6 8.3 %copy-start.6 = (bf16[128,64]{0,1:T(8,128)(2,1)S(1)}, bf16[128,64]{0,1:T(8,128)(2,1)}, u32[]{:S(2)}) copy-start(bf16[128,64]{0,1:T(8,128)(2,1)} %param.15) | copy-start | bytes 49156
  55.6 15.5 %all-to-all-start.2 = ((bf16[16,64,128]{2,1,0:T(8,128)(2,1)}), bf16[16,64,128]{2,1,0:T(8,128)(2,1)S(1)}, u32[]{:S(2)}, u32[]{:S(2)}) async-start(bf16[16,64,128]{2,1,0:T(8,128)(2,1)} %join.1), calls=%async_computation.2 | async-start | bytes 524288 | tf_op jit(solution)/shard_map/all_to_all | solution.py:338
  64.1 9.3 %collective-permute-start.1 = (bf16[64,1664]{1,0:T(8,128)(2,1)S(1)}, bf16[64,1664]{1,0:T(8,128)(2,1)S(1)}, u32[]{:S(2)}, u32[]{:S(2)}) collective-permute-start(bf16[64,1664]{1,0:T(8,128)(2,1)S(1)} %get-tuple-element.30), channel_id=1, source_target_pairs={{0,64},{8,72},{16,80},{24,88},{32,96},{40,104},{48,112},{56,120},{... | collective-permute-start | bytes 638984 | tf_op jit(solution)/shard_map/ppermute | solution.py:382
  74.6 16.6 %all-to-all-start.3 = ((bf16[32,4,1408]{2,1,0:T(4,128)(2,1)}), bf16[32,4,1408]{2,1,0:T(4,128)(2,1)S(1)}, u32[]{:S(2)}, u32[]{:S(2)}) async-start(bf16[32,4,1408]{2,1,0:T(4,128)(2,1)} %get-tuple-element.34), calls=%async_computation.3 | async-start | bytes 720896 | tf_op jit(solution)/shard_map/all_to_all | solution.py:338
  78.4 13.1 %collective-permute-start.2 = (bf16[64,768]{1,0:T(8,128)(2,1)S(1)}, bf16[64,768]{1,0:T(8,128)(2,1)S(1)}, u32[]{:S(2)}, u32[]{:S(2)}) collective-permute-start(bf16[64,768]{1,0:T(8,128)(2,1)S(1)} %get-tuple-element.35), channel_id=1, source_target_pairs={{0,64},{8,72},{16,80},{24,88},{32,96},{40,104},{48,112},{56,120},{... | collective-permute-start | bytes 294920 | tf_op jit(solution)/shard_map/ppermute | solution.py:383
